TPU v7x, 32 devices: a whole 2x2x4 slice. The times are simulated.
32 devices in a mesh: sp: 8 (over z, x), tp: 4 (over y, core).
Axes of the slice: x: 2, y: 2, z: 4, core: 2. Of those that a mesh axis runs over, the one named last changes fastest.
Arguments:
- cotangent: bfloat16 [1536, 2048], P('sp'), may hold values from -8 to 8
- residual: bfloat16 [1536, 2048], P('sp'), may hold values from -6 to 6
- norm_gain: float32 [2048], replicated, may hold values from 0.1 to 1.9
- route_ids: int32 [1536, 2], P('sp'), may hold values from 0 to 7, all different within a row; in each aligned block of 192 rows (0 to 191, 192 to 383, ...) at most 96 rows name the same one
- route_weights: float32 [1536, 2], P('sp'), may hold values from 0.1 to 1
- expert_gate: bfloat16 [8, 2048, 1024], P('sp', None, 'tp'), may hold values from -0.125 to 0.125
- expert_up: bfloat16 [8, 2048, 1024], P('sp', None, 'tp'), may hold values from -0.125 to 0.125
- expert_down: bfloat16 [8, 1024, 2048], P('sp', 'tp'), may hold values from -0.1875 to 0.1875
- out_proj: bfloat16 [2048, 1024], P(None, 'tp'), may hold values from -0.1875 to 0.1875
- conv_out: bfloat16 [1536, 1024], P('sp', 'tp'), may hold values from -6 to 6, as said below
- branch_gate: bfloat16 [1536, 1024], P('sp', 'tp'), may hold values from -6 to 6
- prev_state: bfloat16 [1536, 1024], P('sp', 'tp'), may hold values from -6 to 6
- decay_param: float32 [1024], P('tp'), as said below
- rate_map: bfloat16 [16, 64, 64], P('tp'), may hold values from -0.75 to 0.75
- input_map: bfloat16 [16, 64, 64], P('tp'), may hold values from -0.75 to 0.75
Outputs:
- grad_gate: float32 [8, 2048, 1024], P('sp', None, 'tp')
- grad_up: float32 [8, 2048, 1024], P('sp', None, 'tp')
- grad_down: float32 [8, 1024, 2048], P('sp', 'tp')
- grad_out_proj: float32 [2048, 1024], P('sp', 'tp')
- grad_conv_out: float32 [1536, 1024], P('sp', 'tp')
- grad_branch_gate: float32 [1536, 1024], P('sp', 'tp')
Inputs may be any that keep to these rules, and one draw needn't show every extreme that they name: `route_ids`: within the rows of one device (aligned blocks of 192 rows) no expert is named by more than 96 rows, a bound that some block reaches; the two ids of a row differ. `conv_out`: every entry is a finite value between -6 and 6. `decay_param`: every channel's decay parameter is at least 4.
All inputs are finite; a program needn't handle non-finite values.
Results may differ from a plain program's by a relative error of at most 0.0095.
Values may be sent and summed in bfloat16 or wider, within the bound.
A program may use at most 128 MiB of HBM per device.

v0:
```python
import contextlib

import jax
import jax.numpy as jnp
from jax import lax
from jax.sharding import PartitionSpec as P
from jax.experimental import pallas as pl
from jax.experimental.pallas import tpu as pltpu

RATE_SCALE = 8.0
NORM_EPS = 1e-06
SERIES_EDGE = 0.001
MESH = pl.DeviceIdType.MESH
SCOPES = False
OVER_ROWS = (((0,), (0,)), ((), ()))
OVER_COLS = (((1,), (1,)), ((), ()))


def scope(name):
    return jax.named_scope(name) if SCOPES else contextlib.nullcontext()


def partner_of(place, i, count):
    total = lax.rem(place + i, 2)
    bit = 2
    while bit < count:
        own = lax.div(place, bit) + lax.div(i, bit) + lax.div(i, 2 * bit)
        total = total + bit * lax.rem(own, 2)
        bit *= 2
    return total


def remote(src, dst, send_sem, recv_sem, device):
    return pltpu.make_async_remote_copy(
        src_ref=src,
        dst_ref=dst,
        send_sem=send_sem,
        recv_sem=recv_sem,
        device_id=device,
        device_id_type=MESH,
    )


def one_less_exp(spread):
    small = jnp.minimum(spread, 0.3)
    series = jnp.full_like(small, 1.0 / 40320.0)
    for factorial in (5040.0, 720.0, 120.0, 24.0, 6.0, 2.0, 1.0):
        series = 1.0 / factorial - small * series
    return jnp.where(spread < 0.3, small * series, 1.0 - jnp.exp(-spread))


def loop(begin, end, step):
    def body(i, carry):
        step(i)
        return carry

    lax.fori_loop(begin, end, body, 0)


def layer_kernel(
    sp_count,
    tp_count,
    refs_in,
    gate_grad,
    up_grad,
    down_grad,
    proj_grad,
    conv_grad,
    branch_grad,
    refs_here,
    maps,
    sending,
    moe_part,
    scaled_first,
    scaled_second,
    pre_values,
    held,
    part,
    from_beside,
    to_across,
    from_across,
    mine,
    leaving,
    arrived,
    full,
    hidden,
    d_gate,
    d_up,
    rate_factor,
    input_factor,
    direct_factor,
    gate_factor,
    gelu_values,
    keep,
    branch_all,
    mix,
    share,
    mix_all,
    small,
    small_all,
    load_sem,
    send_sem,
    recv_sem,
    back_send,
    back_recv,
    branch_send,
    branch_recv,
    last_send,
    last_recv,
    share_send,
    share_recv,
    small_send,
    small_recv,
):
    s = lax.axis_index("sp")
    t = lax.axis_index("tp")
    beside = t + 1 - 2 * lax.rem(t, 2)
    across = lax.rem(t + tp_count // 2, tp_count)
    facing = lax.rem(beside + tp_count // 2, tp_count)
    half = sp_count // 2
    s_twin = s + 1 - 2 * lax.rem(s, 2)
    (res, cot, gain, ids, weights, conv, gate, prev, decay, rate_map, input_map) = refs_here[:11]
    gate_w, up_w, down_w, proj = refs_here[11:]
    tok_rows, model_width = res.shape
    cap, width = sending.shape[2:]
    channels = conv.shape[1]
    share_rows, out_rows = share.shape[1:]

    def partner(i):
        return partner_of(s, i, sp_count)

    barrier = pltpu.get_barrier_semaphore()
    for other in (beside, across):
        pl.semaphore_signal(barrier, inc=1, device_id=(s, other), device_id_type=MESH)
    loop(
        1,
        sp_count,
        lambda i: pl.semaphore_signal(
            barrier, inc=1, device_id=(partner(i), t), device_id_type=MESH
        ),
    )
    loads = [
        pltpu.make_async_copy(src, dst, load_sem.at[k])
        for k, (src, dst) in enumerate(zip(refs_in, refs_here))
    ]
    for copy in loads:
        copy.start()
    for copy in loads[:5]:
        copy.wait()

    def cols_of(q):
        return pl.ds(pl.multiple_of(q * width, width), width)

    with scope("prepare"):
        cols = cols_of(t)
        res_all = res[...].astype(jnp.float32)
        inv_rms = lax.rsqrt(jnp.mean(res_all * res_all, axis=1, keepdims=True) + NORM_EPS)
        moe_part[...] = (res[:, cols].astype(jnp.float32) * inv_rms * gain[:, cols]).astype(
            jnp.bfloat16
        )
        square = (tok_rows, tok_rows)
        down_at = lax.broadcasted_iota(jnp.int32, square, 0)
        over_at = lax.broadcasted_iota(jnp.int32, square, 1)

        def column(row):
            return jnp.sum(jnp.where(down_at == over_at, row, 0.0), axis=1, keepdims=True)

        cot_mine = cot[:, cols].astype(jnp.float32)
        scaled_first[...] = (column(weights[0:1, :]) * cot_mine).astype(jnp.bfloat16)
        scaled_second[...] = (column(weights[1:2, :]) * cot_mine).astype(jnp.bfloat16)
        experts = lax.broadcasted_iota(jnp.int32, (sp_count, tok_rows), 0)
        is_first = ids[0:1, :] == experts
        is_second = ids[1:2, :] == experts
        hits = (is_first | is_second).astype(jnp.float32).astype(jnp.bfloat16)
        earlier = (down_at < over_at).astype(jnp.float32).astype(jnp.bfloat16)
        ranks = jnp.dot(hits, earlier, preferred_element_type=jnp.float32)
        row_first = jnp.sum(jnp.where(is_first, ranks, 0.0), axis=0, keepdims=True)
        row_second = jnp.sum(jnp.where(is_second, ranks, 0.0), axis=0, keepdims=True)
        row_first = row_first + (ids[0:1, :] * cap).astype(jnp.float32)
        row_second = row_second + (ids[1:2, :] * cap).astype(jnp.float32)
        slots = lax.broadcasted_iota(jnp.int32, (cap, tok_rows), 0).astype(jnp.float32)

    def filled(target):
        base = (target * cap).astype(jnp.float32)
        first = jnp.where(row_first - base == slots, 1.0, 0.0)
        second = jnp.where(row_second - base == slots, 1.0, 0.0)
        rows = jnp.dot(
            (first + second).astype(jnp.bfloat16),
            moe_part[...],
            preferred_element_type=jnp.float32,
        ).astype(jnp.bfloat16)
        from_first = jnp.dot(
            first.astype(jnp.bfloat16), scaled_first[...], preferred_element_type=jnp.float32
        )
        from_second = jnp.dot(
            second.astype(jnp.bfloat16), scaled_second[...], preferred_element_type=jnp.float32
        )
        return rows, (from_first + from_second).astype(jnp.bfloat16)

    def quarter_of(source, q):
        return held.at[source, :, :, cols_of(q)]

    def first(i):
        target = partner(i)
        return remote(
            sending.at[target], quarter_of(s, t), send_sem.at[0], recv_sem.at[0, i], (target, t)
        )

    def passed(kind, i, q, to):
        block = quarter_of(partner(i), q)
        landing = recv_sem.at[min(kind, 2), i]
        return remote(block, block, send_sem.at[kind], landing, (s, to))

    def landed(i):
        source = partner(i)
        remote(
            sending.at[source],
            quarter_of(source, t),
            send_sem.at[0],
            recv_sem.at[0, i],
            (source, t),
        ).wait_recv()

    def pass_on(i):
        passed(1, i, t, across).start()
        passed(2, i, t, beside).start()

    def pass_back(i):
        passed(1, i, across, across).wait_recv()
        passed(3, i, across, beside).start()

    def all_of(like, sem):
        return remote(like, like, sem, sem, (s, beside))

    def complete(i):
        all_of(sending.at[pl.ds(0, 2)], recv_sem.at[2, i]).wait_recv()

    rows_own, cot_own = filled(s)
    held[s, 0, :, cols] = rows_own
    held[s, 1, :, cols] = cot_own
    with scope("barrier"):
        pl.semaphore_wait(barrier, sp_count + 1)
    pass_on(0)

    def send_one(i):
        target = partner(i)
        rows, values = filled(target)
        sending[target, 0] = rows
        sending[target, 1] = values
        first(i).start()

    early = min(5, sp_count)
    with scope("sends"):
        loop(1, early, send_one)

    for copy in loads[5:11]:
        copy.wait()
    with scope("forward"):
        block = rate_map.shape[1]
        lane_in = lax.rem(lax.broadcasted_iota(jnp.int32, (block, channels), 1), block)
        spread_out = lane_in == lax.broadcasted_iota(jnp.int32, (block, channels), 0)
        spread_out = spread_out.astype(jnp.float32).astype(jnp.bfloat16)
        wide = (channels, channels)
        same = lax.div(lax.broadcasted_iota(jnp.int32, wide, 0), block) == lax.div(
            lax.broadcasted_iota(jnp.int32, wide, 1), block
        )
        for k, blocks in enumerate((rate_map, input_map)):
            tiled = jnp.dot(
                blocks[...].reshape(channels, block),
                spread_out,
                preferred_element_type=jnp.float32,
            )
            maps[:, k * channels : (k + 1) * channels] = jnp.where(same, tiled, 0.0).astype(
                jnp.bfloat16
            )
        pre_values[...] = jnp.dot(conv[...], maps[...], preferred_element_type=jnp.float32)
        y = jnp.exp(-decay[...])
        soft = y * (1.0 - y * (0.5 - y * (1.0 / 3.0 - y * (0.25 - y * 0.2))))
        step = 16

        def forward(i):
            rows = pl.ds(pl.multiple_of(i * step, step), step)
            rate_gate = jax.nn.sigmoid(pre_values[rows, :channels])
            input_gate = jax.nn.sigmoid(pre_values[rows, channels:])
            log_keep = -RATE_SCALE * rate_gate * soft
            kept = jnp.exp(log_keep)
            spread = -2.0 * log_keep
            gone = one_less_exp(spread)
            norm_term = jnp.sqrt(gone)
            conv_values = conv[rows, :].astype(jnp.float32)
            prev_values = prev[rows, :].astype(jnp.float32)
            inner = input_gate * conv_values
            state_now = kept * prev_values + norm_term * inner
            v = gate[rows, :].astype(jnp.float32)
            root = 0.7978845608028654
            bent = jnp.tanh(root * (v + 0.044715 * v * v * v))
            gelu_value = 0.5 * v * (1.0 + bent)
            gelu_slope = 0.5 * (1.0 + bent) + 0.5 * v * (1.0 - bent * bent) * root * (
                1.0 + 3.0 * 0.044715 * v * v
            )
            tiny_side = spread < SERIES_EDGE
            series = jnp.where(
                tiny_side, 1.0 + 0.5 * spread, spread / jnp.where(tiny_side, 1.0, gone)
            )
            slope = 0.5 * jnp.sqrt(spread * series)
            branch_all[s, rows, :] = (state_now * gelu_value).astype(jnp.bfloat16)
            rate_factor[rows, :] = prev_values * kept * (-RATE_SCALE * soft) * rate_gate * (
                1.0 - rate_gate
            ) + inner * kept * kept * (1.0 - rate_gate) * slope
            input_factor[rows, :] = norm_term * conv_values * input_gate * (1.0 - input_gate)
            direct_factor[rows, :] = norm_term * input_gate
            gate_factor[rows, :] = state_now * gelu_slope
            gelu_values[rows, :] = gelu_value
            keep[rows, :] = kept

        loop(0, tok_rows // step, forward)

    for copy in loads[11:]:
        copy.wait()

    def to_beside(i, k):
        source = partner(i)
        q = beside if k == 0 else facing
        return remote(
            part.at[source, :, cols_of(q)],
            from_beside.at[k, source],
            back_send.at[k],
            back_recv.at[k, i],
            (s, beside),
        )

    def crossing(i):
        source = partner(i)
        return remote(
            to_across.at[source],
            from_across.at[source],
            back_send.at[2],
            back_recv.at[2, i],
            (s, across),
        )

    def homeward(i):
        source = partner(i)
        return remote(
            leaving.at[source],
            arrived.at[s],
            back_send.at[3],
            back_recv.at[3, i],
            (source, t),
        )

    def expert(i):
        complete(i)
        source = partner(i)
        rows_in = held[source, 0]
        gate_pre = jnp.dot(rows_in, gate_w[...], preferred_element_type=jnp.float32)
        up_pre = jnp.dot(rows_in, up_w[...], preferred_element_type=jnp.float32)
        d_hidden = lax.dot_general(
            held[source, 1], down_w[...], OVER_COLS, preferred_element_type=jnp.float32
        )
        gate_sig = jax.nn.sigmoid(gate_pre)
        gate_act = gate_pre * gate_sig
        up_back = (d_hidden * gate_act).astype(jnp.bfloat16)
        gate_back = (d_hidden * up_pre * gate_sig * (1.0 + gate_pre * (1.0 - gate_sig))).astype(
            jnp.bfloat16
        )
        hidden[source] = (gate_act * up_pre).astype(jnp.bfloat16)
        d_up[source] = up_back
        d_gate[source] = gate_back
        back = lax.dot_general(
            gate_back, gate_w[...], OVER_COLS, preferred_element_type=jnp.float32
        )
        back = back + lax.dot_general(
            up_back, up_w[...], OVER_COLS, preferred_element_type=jnp.float32
        )
        part[source] = back.astype(jnp.bfloat16)
        to_beside(i, 1).start()
        to_beside(i, 0).start()

    def cross(i):
        to_beside(i, 1).wait_recv()
        at = partner(i)
        total = part[at, :, cols_of(across)].astype(jnp.float32) + from_beside[1, at].astype(
            jnp.float32
        )
        to_across[at] = total.astype(jnp.bfloat16)
        crossing(i).start()
        to_beside(i, 0).wait_recv()
        mine[at] = part[at, :, cols].astype(jnp.float32) + from_beside[0, at].astype(jnp.float32)

    def leave(i):
        crossing(i).wait_recv()
        at = partner(i)
        total = (mine[at] + from_across[at].astype(jnp.float32)).astype(jnp.bfloat16)

        @pl.when(i > 0)
        def _():
            leaving[at] = total
            homeward(i).start()

        @pl.when(i == 0)
        def _():
            arrived[s] = total

    def turn(i):
        @pl.when((i >= 2) & (i < sp_count + 2))
        def _():
            with scope("expert"):
                expert(i - 2)

        @pl.when(i >= 4)
        def _():
            with scope("leave"):
                leave(i - 4)

        @pl.when((i >= 1) & (i < sp_count))
        def _():
            with scope("landed"):
                landed(i)
            pass_on(i)

        @pl.when((i >= 1) & (i + early - 1 < sp_count))
        def _():
            send_one(i + early - 1)

        @pl.when((i >= 1) & (i < sp_count + 1))
        def _():
            with scope("pass_back"):
                pass_back(i - 1)

        @pl.when((i >= 2) & (i < sp_count + 2))
        def _():
            with scope("cross"):
                cross(i - 2)

    loop(0, sp_count + 4, turn)

    own_branch = branch_all.at[s]

    def branch_copy(j):
        return remote(
            own_branch,
            own_branch,
            branch_send.at[0],
            branch_recv.at[j],
            (partner(2 * j), t),
        )

    def branch_landed(j):
        source = partner(2 * j)
        return remote(
            own_branch,
            branch_all.at[source],
            branch_send.at[0],
            branch_recv.at[j],
            (source, t),
        )

    def branch_twin(j):
        block = branch_all.at[partner(2 * j)]
        return remote(block, block, branch_send.at[1], branch_recv.at[0], (s_twin, t))

    def merged(values):
        return values.reshape(sp_count * cap, values.shape[2])

    def summed(left, right):
        if cap % 16 == 0:
            return lax.dot_general(
                merged(left), merged(right), OVER_ROWS, preferred_element_type=jnp.float32
            )
        total = None
        for source in range(sp_count):
            one = lax.dot_general(
                left[source], right[source], OVER_ROWS, preferred_element_type=jnp.float32
            )
            total = one if total is None else total + one
        return total

    tile = 256
    def rows_tile(k):
        at = pl.ds(pl.multiple_of(k * tile, tile), tile)
        rows = held[:, 0, :, at]
        gate_grad[at, :] = summed(rows, d_gate[...])
        up_grad[at, :] = summed(rows, d_up[...])

    def cot_tile(k):
        at = pl.ds(pl.multiple_of(k * tile, tile), tile)
        down_grad[:, at] = summed(hidden[...], held[:, 1, :, at])

    with scope("grads_rows"):
        loop(0, model_width // tile, rows_tile)

    lanes = lax.broadcasted_iota(jnp.int32, (tok_rows, cap), 1).astype(jnp.float32)
    slot_first, slot_second = column(row_first), column(row_second)

    def gather_rows(source):
        base = (source * cap).astype(jnp.float32)
        chosen = jnp.where(slot_first - base == lanes, 1.0, 0.0)
        chosen = chosen + jnp.where(slot_second - base == lanes, 1.0, 0.0)
        return jnp.dot(
            chosen.astype(jnp.bfloat16), arrived[source], preferred_element_type=jnp.float32
        )

    def add_in(i, total):
        source = partner(i)
        with scope("home"):
            remote(
                leaving.at[source],
                arrived.at[source],
                back_send.at[3],
                back_recv.at[3, i],
                (source, t),
            ).wait_recv()
        return total + gather_rows(source)

    full[:, cols] = lax.fori_loop(1, sp_count, add_in, gather_rows(s)).astype(jnp.bfloat16)

    def gathered(kind, q, to):
        block = full.at[:, cols_of(q)]
        return remote(block, block, last_send.at[kind], last_recv.at[kind], (s, to))

    gathered(0, t, across).start()
    gathered(1, t, beside).start()
    loop(1, half, lambda j: branch_copy(j).start())
    branch_twin(0).start()
    with scope("grads_cot"):
        loop(0, model_width // tile, cot_tile)
    with scope("quarter"):
        gathered(0, across, across).wait_recv()
        gathered(2, across, beside).start()
        gathered(1, beside, beside).wait_recv()
        gathered(2, facing, beside).wait_recv()

    def mix_rows(begin):
        rows = pl.ds(pl.multiple_of(begin, share_rows), share_rows)
        values = res[rows, :].astype(jnp.float32)
        weighted = gain[...] * full[rows, :].astype(jnp.float32)
        inverse = lax.rsqrt(jnp.mean(values * values, axis=1, keepdims=True) + NORM_EPS)
        cubed = inverse * inverse * inverse
        slope = cubed * jnp.mean(values * weighted, axis=1, keepdims=True)
        return rows, (
            cot[rows, :].astype(jnp.float32) + inverse * weighted - values * slope
        ).astype(jnp.bfloat16)

    def share_view(source, q):
        return mix_all.at[source, pl.ds(pl.multiple_of(q * share_rows, share_rows), share_rows), :]

    def share_first(i):
        target = partner(i)
        return remote(
            share.at[target],
            share_view(s, t),
            share_send.at[0],
            share_recv.at[0, i],
            (target, t),
        )

    def share_passed(kind, i, q, to):
        block = share_view(partner(i), q)
        landing = share_recv.at[1, i] if kind == 1 else share_recv.at[0, 0]
        return remote(block, block, share_send.at[kind], landing, (s, to))

    def share_landed(i):
        source = partner(i)
        remote(
            share.at[source],
            share_view(source, t),
            share_send.at[0],
            share_recv.at[0, i],
            (source, t),
        ).wait_recv()

    def share_on(i):
        share_passed(1, i, t, across).start()
        share_passed(2, i, t, beside).start()

    def share_back(i):
        share_passed(1, i, across, across).wait_recv()
        share_passed(3, i, across, beside).start()

    with scope("share"):
        _, own_rows = mix_rows(t * share_rows)
        for j in range(sp_count):
            share[j] = own_rows[:, j * out_rows : (j + 1) * out_rows]
        loop(1, sp_count, lambda i: share_first(i).start())
        own_at = pl.ds(pl.multiple_of(t * share_rows, share_rows), share_rows)
        mix_all[s, own_at, :] = share[s]
        share_on(0)

    with scope("branch_pass"):

        def pass_branch(j):
            branch_landed(j).wait_recv()
            branch_twin(j).start()

        loop(1, half, pass_branch)
    with scope("mix"):

        def fill(k):
            rows, values = mix_rows(k * share_rows)
            mix[rows, :] = values

        loop(0, tp_count, fill)

    with scope("scan"):
        d_branch = jnp.dot(mix[...], proj[...], preferred_element_type=jnp.float32)
        branch_grad[...] = d_branch * gate_factor[...]
        at = lax.broadcasted_iota(jnp.int32, d_branch.shape, 0)
        grads = d_branch * gelu_values[...]
        keeps = jnp.where(at < tok_rows - 1, pltpu.roll(keep[...], tok_rows - 1, 0), 1.0)
        reach = 1
        while reach < tok_rows:
            inside = at < tok_rows - reach
            later_grads = jnp.where(inside, pltpu.roll(grads, tok_rows - reach, 0), 0.0)
            later_keeps = jnp.where(inside, pltpu.roll(keeps, tok_rows - reach, 0), 1.0)
            grads = grads + keeps * later_grads
            keeps = keeps * later_keeps
            reach *= 2
        small[...] = jnp.zeros_like(small)
        small[0:1, :] = keep[0:1, :] * keeps[0:1, :]
        small[1:2, :] = keep[0:1, :] * grads[0:1, :]
        small_all[s] = jnp.zeros(small.shape, jnp.float32)

    def carry_to(i):
        return remote(
            small, small_all.at[s], small_send.at[0], small_recv.at[0], (partner(i), t)
        )

    loop(1, sp_count, lambda i: carry_to(i).start())

    def relay(i):
        @pl.when(i < sp_count)
        def _():
            share_landed(i)
            share_on(i)

        @pl.when(i >= 2)
        def _():
            share_back(i - 2)

    with scope("relay"):
        loop(1, sp_count + 2, relay)

    with scope("small"):
        all_of(small_all.at[pl.ds(0, sp_count - 1)], small_recv.at[0]).wait_recv()

    def compose(turn, carried):
        source = sp_count - 1 - turn
        later = small_all[source]
        return jnp.where(source > s, later[1:2] + later[0:1] * carried, carried)

    with scope("back_maps"):
        carried = lax.fori_loop(0, sp_count - 1, compose, jnp.zeros((1, channels), jnp.float32))
        state_grad = grads + keeps * carried
        back = jnp.concatenate(
            [state_grad * rate_factor[...], state_grad * input_factor[...]], axis=1
        )
        high = back.astype(jnp.bfloat16)
        low = (back - high.astype(jnp.float32)).astype(jnp.bfloat16)
        conv_grad[...] = (
            state_grad * direct_factor[...]
            + lax.dot_general(high, maps[...], OVER_COLS, preferred_element_type=jnp.float32)
            + lax.dot_general(low, maps[...], OVER_COLS, preferred_element_type=jnp.float32)
        )

    with scope("last_waits"):

        all_of(mix_all.at[:, pl.ds(0, 2 * share_rows)], share_recv.at[0, 0]).wait_recv()
        all_of(branch_all.at[pl.ds(0, half)], branch_recv.at[0]).wait_recv()
    with scope("grad_proj"):
        proj_grad[...] = lax.dot_general(
            mix_all[...].reshape(sp_count * tok_rows, out_rows),
            branch_all[...].reshape(sp_count * tok_rows, channels),
            OVER_ROWS,
            preferred_element_type=jnp.float32,
        )

    others = pl.ds(0, sp_count - 1)
    with scope("end"):
        all_of(sending.at[others], send_sem.at[0]).wait_send()
        for kind in (1, 2, 3):
            all_of(sending, send_sem.at[kind]).wait_send()
            all_of(to_across, back_send.at[kind - 1]).wait_send()
            all_of(share, share_send.at[kind]).wait_send()
        all_of(to_across.at[others], back_send.at[3]).wait_send()
        all_of(share.at[others], share_send.at[0]).wait_send()
        all_of(small_all.at[others], small_send.at[0]).wait_send()
        all_of(branch_all.at[pl.ds(0, half - 1)], branch_send.at[0]).wait_send()
        all_of(branch_all.at[pl.ds(0, half)], branch_send.at[1]).wait_send()
        gathered(0, t, across).wait_send()
        gathered(1, t, beside).wait_send()
        gathered(2, across, beside).wait_send()


def layer(sp_count, tp_count, cap, operands):
    res, conv, gate_w, down_w = (operands[k] for k in (0, 5, 11, 13))
    tok_rows, model_width = res.shape
    channels, units = conv.shape[1], down_w.shape[0]
    width = model_width // tp_count
    share_rows, out_rows = tok_rows // tp_count, model_width // sp_count
    vmem = pl.BlockSpec(memory_space=pltpu.VMEM)
    anywhere = pl.BlockSpec(memory_space=pl.ANY)
    low, exact = jnp.bfloat16, jnp.float32
    blocks = (sp_count, cap, width)
    scratch = [
        ((channels, 2 * channels), low),
        ((sp_count, 2, cap, width), low),
        ((tok_rows, width), low),
        ((tok_rows, width), low),
        ((tok_rows, width), low),
        ((tok_rows, 2 * channels), exact),
        ((sp_count, 2, cap, model_width), low),
        ((sp_count, cap, model_width), low),
        ((2,) + blocks, low),
        (blocks, low),
        (blocks, low),
        (blocks, exact),
        (blocks, low),
        (blocks, low),
        (res.shape, low),
        ((sp_count, cap, units), low),
        ((sp_count, cap, units), low),
        ((sp_count, cap, units), low),
    ]
    scratch += [(conv.shape, exact)] * 6
    scratch += [
        ((sp_count,) + conv.shape, low),
        (res.shape, low),
        ((sp_count, share_rows, out_rows), low),
        ((sp_count, tok_rows, out_rows), low),
        ((8, channels), exact),
        ((sp_count, 8, channels), exact),
    ]
    sems = [
        (len(operands),),
        (4,),
        (3, sp_count),
        (4,),
        (4, sp_count),
        (2,),
        (sp_count // 2,),
        (3,),
        (3,),
        (4,),
        (2, sp_count),
        (1,),
        (1,),
    ]
    def grouped(*refs):
        layer_kernel(sp_count, tp_count, refs[: len(operands)], *refs[len(operands) :])

    return pl.pallas_call(
        grouped,
        out_shape=[
            pltpu.VMEM(shape, exact)
            for shape in (
                gate_w.shape,
                gate_w.shape,
                down_w.shape,
                (out_rows, channels),
                conv.shape,
                conv.shape,
            )
        ],
        in_specs=[anywhere] * len(operands),
        out_specs=[vmem] * 6,
        scratch_shapes=[[pltpu.VMEM(given.shape, given.dtype) for given in operands]]
        + [pltpu.VMEM(shape, kind) for shape, kind in scratch]
        + [pltpu.SemaphoreType.DMA(shape) for shape in sems],
        compiler_params=pltpu.CompilerParams(collective_id=1, has_side_effects=True, vmem_limit_bytes=59_000_000),
        cost_estimate=pl.CostEstimate(flops=0, bytes_accessed=40_000_000, transcendentals=0),
    )(*operands)


def store_kernel(*refs):
    count = len(refs) // 2
    sems = refs[-1]
    copies = [
        pltpu.make_async_copy(refs[k], refs[count + k], sems.at[k]) for k in range(count)
    ]
    for copy in copies:
        copy.start()
    for copy in copies:
        copy.wait()


def store(values):
    return pl.pallas_call(
        store_kernel,
        out_shape=[jax.ShapeDtypeStruct(value.shape, value.dtype) for value in values],
        in_specs=[pl.BlockSpec(memory_space=pltpu.VMEM)] * len(values),
        out_specs=[pl.BlockSpec(memory_space=pl.ANY)] * len(values),
        scratch_shapes=[pltpu.SemaphoreType.DMA((len(values),))],
        compiler_params=pltpu.CompilerParams(vmem_limit_bytes=16 * 1024 * 1024),
    )(*[pltpu.with_memory_space_constraint(value, pltpu.VMEM) for value in values])


def per_device(
    cotangent,
    residual,
    norm_gain,
    route_ids,
    route_weights,
    expert_gate,
    expert_up,
    expert_down,
    out_proj,
    conv_out,
    branch_gate,
    prev_state,
    decay_param,
    rate_map,
    input_map,
):
    sp_count = lax.axis_size("sp")
    tp_count = lax.axis_size("tp")
    experts_all = expert_gate.shape[0] * sp_count
    capacity = 4 * residual.shape[0] // experts_all
    grads = layer(
        sp_count,
        tp_count,
        capacity,
        (
            residual,
            cotangent,
            norm_gain[None, :],
            route_ids.T,
            route_weights.T,
            conv_out,
            branch_gate,
            prev_state,
            decay_param[None, :],
            rate_map,
            input_map,
            expert_gate[0],
            expert_up[0],
            expert_down[0],
            out_proj,
        ),
    )
    grad_gate, grad_up, grad_down, grad_out_proj, grad_conv_out, grad_branch_gate = store(grads)
    return (
        grad_gate[None],
        grad_up[None],
        grad_down[None],
        grad_out_proj,
        grad_conv_out,
        grad_branch_gate,
    )


def solution(mesh):
    in_specs = (
        P("sp", None),
        P("sp", None),
        P(),
        P("sp", None),
        P("sp", None),
        P("sp", None, "tp"),
        P("sp", None, "tp"),
        P("sp", "tp", None),
        P(None, "tp"),
        P("sp", "tp"),
        P("sp", "tp"),
        P("sp", "tp"),
        P("tp"),
        P("tp", None, None),
        P("tp", None, None),
    )
    out_specs = (
        P("sp", None, "tp"),
        P("sp", None, "tp"),
        P("sp", "tp", None),
        P("sp", "tp"),
        P("sp", "tp"),
        P("sp", "tp"),
    )
    return jax.shard_map(
        per_device, mesh=mesh, in_specs=in_specs, out_specs=out_specs, check_vma=False
    )
```

profile of v0, /device:TPU:0, one launch (start us, length us, event | category | flops | bytes accessed | tf_op | source)
XLA Modules:
  0.0 96.3 jit_solution(9682488533967706130)
XLA Ops:
  0.6 92.7 %shard_map.190 = (f32[2048,256]{1,0:T(8,128)S(1)}, f32[2048,256]{1,0:T(8,128)S(1)}, f32[256,2048]{1,0:T(8,128)S(1)}, f32[256,256]{1,0:T(8,128)S(1)}, f32[192,256]{1,0:T(8,128)S(1)}, /*index=5*/f32[192,256]{1,0:T(8,128)S(1)}) custom-call(bf16[192,2048]{1,0:T(8,128)(2,1)} %refs_0_.1, bf16[192,2048]{1,0:T(8,128)(2,1)} %refs_1_.1, f32[1,2048]{1,0:T(1,128)} %bitcast.13, ...), custom_call_target="tpu_custom_call" | custom-call | bytes 40000000 | tf_op jit(solution)/shard_map/pallas_call | solution.py:752
  93.4 2.9 %shard_map.191 = (f32[2048,256]{1,0:T(8,128)}, f32[2048,256]{1,0:T(8,128)}, f32[256,2048]{1,0:T(8,128)}, f32[256,256]{1,0:T(8,128)}, f32[192,256]{1,0:T(8,128)}, /*index=5*/f32[192,256]{1,0:T(8,128)}) custom-call(f32[2048,256]{1,0:T(8,128)S(1)} %get-tuple-element.18.refs_0_, f32[2048,256]{1,0:T(8,128)S(1)} %get-tuple-element.19.refs_1_, ...), custom_call_target="tpu_custom_call" | custom-call | tf_op jit(solution)/shard_map/pallas_call | solution.py:788
where the time goes:
time: 96.7 us; the launch traced here: 96.3 us
  Pallas kernels  95.6 us (99%)
    pallas_call x1, Pallas kernels, layer(): pl.pallas_call(grouped, out_shape=[pltpu.VMEM(shape, exact) for shape in...  92.7 us
    pallas_call x1, Pallas kernels, store(): pl.pallas_call(store_kernel, out_shape=[jax.ShapeDtypeStruct(value.shape,...  2.88 us

commit v1 on v0

--- a/solution.py
+++ b/solution.py
@@ -377,14 +377,15 @@
         to_beside(i, 1).start()
         to_beside(i, 0).start()
 
-    def cross(i):
+    def cross(i, at_once):
         to_beside(i, 1).wait_recv()
         at = partner(i)
         total = part[at, :, cols_of(across)].astype(jnp.float32) + from_beside[1, at].astype(
             jnp.float32
         )
         to_across[at] = total.astype(jnp.bfloat16)
-        crossing(i).start()
+        if at_once:
+            crossing(i).start()
         to_beside(i, 0).wait_recv()
         mine[at] = part[at, :, cols].astype(jnp.float32) + from_beside[0, at].astype(jnp.float32)
 
@@ -392,48 +393,11 @@
         crossing(i).wait_recv()
         at = partner(i)
         total = (mine[at] + from_across[at].astype(jnp.float32)).astype(jnp.bfloat16)
-
-        @pl.when(i > 0)
-        def _():
+        if isinstance(i, int) and i == 0:
+            arrived[s] = total
+        else:
             leaving[at] = total
             homeward(i).start()
-
-        @pl.when(i == 0)
-        def _():
-            arrived[s] = total
-
-    def turn(i):
-        @pl.when((i >= 2) & (i < sp_count + 2))
-        def _():
-            with scope("expert"):
-                expert(i - 2)
-
-        @pl.when(i >= 4)
-        def _():
-            with scope("leave"):
-                leave(i - 4)
-
-        @pl.when((i >= 1) & (i < sp_count))
-        def _():
-            with scope("landed"):
-                landed(i)
-            pass_on(i)
-
-        @pl.when((i >= 1) & (i + early - 1 < sp_count))
-        def _():
-            send_one(i + early - 1)
-
-        @pl.when((i >= 1) & (i < sp_count + 1))
-        def _():
-            with scope("pass_back"):
-                pass_back(i - 1)
-
-        @pl.when((i >= 2) & (i < sp_count + 2))
-        def _():
-            with scope("cross"):
-                cross(i - 2)
-
-    loop(0, sp_count + 4, turn)
 
     own_branch = branch_all.at[s]
 
@@ -459,6 +423,83 @@
     def branch_twin(j):
         block = branch_all.at[partner(2 * j)]
         return remote(block, block, branch_send.at[1], branch_recv.at[0], (s_twin, t))
+
+    near = 4
+    stride = 3 if sp_count == 8 else 2
+    lag = 3 - stride
+
+    def turn(i):
+        @pl.when((i >= 2) & (i < sp_count + 2))
+        def _():
+            with scope("expert"):
+                expert(i - 2)
+
+        @pl.when((i >= near + 2) & (i < sp_count + 2))
+        def _():
+            with scope("cross"):
+                cross(i - 2, True)
+
+        @pl.when(i == sp_count)
+        def _():
+            crossing(2).start()
+            crossing(3).start()
+
+        @pl.when(i >= near + 3)
+        def _():
+            with scope("leave"):
+                leave(i - 3)
+
+        @pl.when(i == near + 3)
+        def _():
+            leave(0)
+            leave(1)
+
+        @pl.when(i == sp_count + 1)
+        def _():
+            leave(2)
+            leave(3)
+
+        @pl.when((i >= 1) & (i < sp_count))
+        def _():
+            with scope("landed"):
+                landed(i)
+            pass_on(i)
+
+        @pl.when(i == 1)
+        def _():
+            branch_twin(0).start()
+
+        @pl.when((i >= 3) & (i <= stride * (half - 2) + lag) & (lax.rem(i - lag, stride) == 0))
+        def _():
+            branch_copy(lax.div(i - lag, stride)).start()
+
+        @pl.when((i >= 1) & (i + early - 1 < sp_count))
+        def _():
+            send_one(i + early - 1)
+
+        @pl.when(i == near + 1)
+        def _():
+            crossing(0).start()
+            crossing(1).start()
+
+        @pl.when((i >= 1) & (i < sp_count + 1))
+        def _():
+            with scope("pass_back"):
+                pass_back(i - 1)
+
+        @pl.when((i >= 2) & (i < near + 2))
+        def _():
+            with scope("cross"):
+                cross(i - 2, False)
+
+    loop(0, sp_count + 3, turn)
+
+    def pass_branch(j):
+        branch_landed(j).wait_recv()
+        branch_twin(j).start()
+
+    with scope("branch_pass"):
+        loop(1, half - 1, pass_branch)
 
     def merged(values):
         return values.reshape(sp_count * cap, values.shape[2])
@@ -515,21 +556,25 @@
 
     full[:, cols] = lax.fori_loop(1, sp_count, add_in, gather_rows(s)).astype(jnp.bfloat16)
 
-    def gathered(kind, q, to):
-        block = full.at[:, cols_of(q)]
-        return remote(block, block, last_send.at[kind], last_recv.at[kind], (s, to))
-
-    gathered(0, t, across).start()
-    gathered(1, t, beside).start()
-    loop(1, half, lambda j: branch_copy(j).start())
-    branch_twin(0).start()
+    pair, other_pair = lax.div(t, 2), lax.div(across, 2)
+
+    def gathered(kind, part_of, q, to, late):
+        rows = pl.ds(pl.multiple_of(part_of * 2 * share_rows, 2 * share_rows), 2 * share_rows)
+        block = full.at[rows, cols_of(q)]
+        return remote(block, block, last_send.at[kind, late], last_recv.at[kind, late], (s, to))
+
+    gathered(0, other_pair, t, across, 0).start()
+    gathered(1, pair, t, beside, 0).start()
+    gathered(0, pair, t, across, 1).start()
+    gathered(1, other_pair, t, beside, 1).start()
+    branch_copy(half - 1).start()
     with scope("grads_cot"):
         loop(0, model_width // tile, cot_tile)
     with scope("quarter"):
-        gathered(0, across, across).wait_recv()
-        gathered(2, across, beside).start()
-        gathered(1, beside, beside).wait_recv()
-        gathered(2, facing, beside).wait_recv()
+        gathered(0, pair, across, across, 0).wait_recv()
+        gathered(2, pair, across, beside, 0).start()
+        gathered(1, pair, beside, beside, 0).wait_recv()
+        gathered(2, pair, facing, beside, 0).wait_recv()
 
     def mix_rows(begin):
         rows = pl.ds(pl.multiple_of(begin, share_rows), share_rows)
@@ -582,18 +627,17 @@
         _, own_rows = mix_rows(t * share_rows)
         for j in range(sp_count):
             share[j] = own_rows[:, j * out_rows : (j + 1) * out_rows]
-        loop(1, sp_count, lambda i: share_first(i).start())
+        loop(1, sp_count, lambda i: share_first(sp_count - i).start())
         own_at = pl.ds(pl.multiple_of(t * share_rows, share_rows), share_rows)
         mix_all[s, own_at, :] = share[s]
         share_on(0)
 
-    with scope("branch_pass"):
-
-        def pass_branch(j):
-            branch_landed(j).wait_recv()
-            branch_twin(j).start()
-
-        loop(1, half, pass_branch)
+    with scope("quarter_late"):
+        gathered(0, other_pair, across, across, 1).wait_recv()
+        gathered(2, other_pair, across, beside, 1).start()
+        gathered(1, other_pair, beside, beside, 1).wait_recv()
+        gathered(2, other_pair, facing, beside, 1).wait_recv()
+
     with scope("mix"):
 
         def fill(k):
@@ -628,6 +672,9 @@
 
     loop(1, sp_count, lambda i: carry_to(i).start())
 
+    with scope("branch_last"):
+        pass_branch(half - 1)
+
     def relay(i):
         @pl.when(i < sp_count)
         def _():
@@ -687,9 +734,10 @@
         all_of(small_all.at[others], small_send.at[0]).wait_send()
         all_of(branch_all.at[pl.ds(0, half - 1)], branch_send.at[0]).wait_send()
         all_of(branch_all.at[pl.ds(0, half)], branch_send.at[1]).wait_send()
-        gathered(0, t, across).wait_send()
-        gathered(1, t, beside).wait_send()
-        gathered(2, across, beside).wait_send()
+        for late, (near_half, far_half) in enumerate(((pair, other_pair), (other_pair, pair))):
+            gathered(0, far_half, t, across, late).wait_send()
+            gathered(1, near_half, t, beside, late).wait_send()
+            gathered(2, near_half, across, beside, late).wait_send()
 
 
 def layer(sp_count, tp_count, cap, operands):
@@ -739,8 +787,8 @@
         (4, sp_count),
         (2,),
         (sp_count // 2,),
-        (3,),
-        (3,),
+        (3, 2),
+        (3, 2),
         (4,),
         (2, sp_count),
         (1,),

time: 96.7 us -> 91.6 us (0.947)
  Pallas kernels: 95.6 us -> 90.5 us
    pallas_call x1, Pallas kernels: 92.7 us -> 87.6 us  [layer(): pl.pallas_call(grouped, out_shape=[pltpu.VMEM(shape, exact) for shape in...]
where the time goes in v1:
time: 91.6 us; the launch traced here: 91.1 us
  Pallas kernels  90.5 us (99%)
    pallas_call x1, Pallas kernels, layer(): pl.pallas_call(grouped, out_shape=[pltpu.VMEM(shape, exact) for shape in...  87.6 us
    pallas_call x1, Pallas kernels, store(): pl.pallas_call(store_kernel, out_shape=[jax.ShapeDtypeStruct(value.shape,...  2.88 us

profile of v1, /device:TPU:0, one launch (start us, length us, event | category | flops | bytes accessed | tf_op | source)
XLA Modules:
  0.0 91.1 jit_solution(15082815995864039916)
XLA Ops:
  0.6 87.6 %shard_map.190 = (f32[2048,256]{1,0:T(8,128)S(1)}, f32[2048,256]{1,0:T(8,128)S(1)}, f32[256,2048]{1,0:T(8,128)S(1)}, f32[256,256]{1,0:T(8,128)S(1)}, f32[192,256]{1,0:T(8,128)S(1)}, /*index=5*/f32[192,256]{1,0:T(8,128)S(1)}) custom-call(bf16[192,2048]{1,0:T(8,128)(2,1)} %refs_0_.1, bf16[192,2048]{1,0:T(8,128)(2,1)} %refs_1_.1, f32[1,2048]{1,0:T(1,128)} %bitcast.13, ...), custom_call_target="tpu_custom_call" | custom-call | bytes 40000000 | tf_op jit(solution)/shard_map/pallas_call | solution.py:800
  88.2 2.9 %shard_map.191 = (f32[2048,256]{1,0:T(8,128)}, f32[2048,256]{1,0:T(8,128)}, f32[256,2048]{1,0:T(8,128)}, f32[256,256]{1,0:T(8,128)}, f32[192,256]{1,0:T(8,128)}, /*index=5*/f32[192,256]{1,0:T(8,128)}) custom-call(f32[2048,256]{1,0:T(8,128)S(1)} %get-tuple-element.18.refs_0_, f32[2048,256]{1,0:T(8,128)S(1)} %get-tuple-element.19.refs_1_, ...), custom_call_target="tpu_custom_call" | custom-call | tf_op jit(solution)/shard_map/pallas_call | solution.py:836

commit v2 on v1

--- a/solution.py
+++ b/solution.py
@@ -558,23 +558,55 @@
 
     pair, other_pair = lax.div(t, 2), lax.div(across, 2)
 
-    def gathered(kind, part_of, q, to, late):
-        rows = pl.ds(pl.multiple_of(part_of * 2 * share_rows, 2 * share_rows), 2 * share_rows)
+    def rows_of(q):
+        return pl.ds(pl.multiple_of(q * share_rows, share_rows), share_rows)
+
+    def pair_rows(p):
+        return pl.ds(pl.multiple_of(p * 2 * share_rows, 2 * share_rows), 2 * share_rows)
+
+    def given(kind, rows, q, to):
         block = full.at[rows, cols_of(q)]
-        return remote(block, block, last_send.at[kind, late], last_recv.at[kind, late], (s, to))
-
-    gathered(0, other_pair, t, across, 0).start()
-    gathered(1, pair, t, beside, 0).start()
-    gathered(0, pair, t, across, 1).start()
-    gathered(1, other_pair, t, beside, 1).start()
+        return remote(block, block, last_send.at[kind], last_recv.at[kind], (s, to))
+
+    def own_first(kind, mine_too):
+        peer = (across, beside, facing)[kind]
+        return given(kind, rows_of(t), peer, peer) if mine_too else given(kind, rows_of(peer), t, peer)
+
+    for kind in (2, 0, 1):
+        own_first(kind, False).start()
+
+    def rest_across(at_peer):
+        if at_peer:
+            return (
+                given(3, pair_rows(other_pair), across, across),
+                given(4, rows_of(beside), across, across),
+            )
+        return given(3, pair_rows(pair), t, across), given(4, rows_of(facing), t, across)
+
+    def rest_beside(at_peer):
+        if at_peer:
+            return (
+                given(5, pair_rows(other_pair), beside, beside),
+                given(6, rows_of(beside), beside, beside),
+            )
+        return given(5, pair_rows(other_pair), t, beside), given(6, rows_of(t), t, beside)
+
+    def rest_facing(at_peer):
+        if at_peer:
+            return (
+                given(7, pair_rows(other_pair), facing, beside),
+                given(8, rows_of(beside), facing, beside),
+            )
+        return given(7, pair_rows(other_pair), across, beside), given(8, rows_of(t), across, beside)
+
+    for copy in rest_across(False) + rest_beside(False):
+        copy.start()
     branch_copy(half - 1).start()
     with scope("grads_cot"):
         loop(0, model_width // tile, cot_tile)
     with scope("quarter"):
-        gathered(0, pair, across, across, 0).wait_recv()
-        gathered(2, pair, across, beside, 0).start()
-        gathered(1, pair, beside, beside, 0).wait_recv()
-        gathered(2, pair, facing, beside, 0).wait_recv()
+        for kind in range(3):
+            own_first(kind, True).wait_recv()
 
     def mix_rows(begin):
         rows = pl.ds(pl.multiple_of(begin, share_rows), share_rows)
@@ -615,13 +647,23 @@
             (source, t),
         ).wait_recv()
 
+    straight = 5 * sp_count // 8
+
     def share_on(i):
         share_passed(1, i, t, across).start()
+
+        @pl.when(i >= straight)
+        def _():
+            share_passed(3, i, t, facing).start()
+
         share_passed(2, i, t, beside).start()
 
     def share_back(i):
         share_passed(1, i, across, across).wait_recv()
-        share_passed(3, i, across, beside).start()
+
+        @pl.when(i < straight)
+        def _():
+            share_passed(3, i, across, beside).start()
 
     with scope("share"):
         _, own_rows = mix_rows(t * share_rows)
@@ -633,10 +675,19 @@
         share_on(0)
 
     with scope("quarter_late"):
-        gathered(0, other_pair, across, across, 1).wait_recv()
-        gathered(2, other_pair, across, beside, 1).start()
-        gathered(1, other_pair, beside, beside, 1).wait_recv()
-        gathered(2, other_pair, facing, beside, 1).wait_recv()
+        for copy in rest_across(True):
+            copy.wait_recv()
+        for copy in rest_facing(False):
+            copy.start()
+        for copy in rest_beside(True) + rest_facing(True):
+            copy.wait_recv()
+
+    def relay(i):
+        share_landed(i)
+        share_on(i)
+
+    with scope("relay"):
+        loop(1, sp_count, relay)
 
     with scope("mix"):
 
@@ -675,18 +726,8 @@
     with scope("branch_last"):
         pass_branch(half - 1)
 
-    def relay(i):
-        @pl.when(i < sp_count)
-        def _():
-            share_landed(i)
-            share_on(i)
-
-        @pl.when(i >= 2)
-        def _():
-            share_back(i - 2)
-
-    with scope("relay"):
-        loop(1, sp_count + 2, relay)
+    with scope("relay_back"):
+        loop(0, sp_count, share_back)
 
     with scope("small"):
         all_of(small_all.at[pl.ds(0, sp_count - 1)], small_recv.at[0]).wait_recv()
@@ -734,10 +775,10 @@
         all_of(small_all.at[others], small_send.at[0]).wait_send()
         all_of(branch_all.at[pl.ds(0, half - 1)], branch_send.at[0]).wait_send()
         all_of(branch_all.at[pl.ds(0, half)], branch_send.at[1]).wait_send()
-        for late, (near_half, far_half) in enumerate(((pair, other_pair), (other_pair, pair))):
-            gathered(0, far_half, t, across, late).wait_send()
-            gathered(1, near_half, t, beside, late).wait_send()
-            gathered(2, near_half, across, beside, late).wait_send()
+        for kind in range(3):
+            own_first(kind, False).wait_send()
+        for copy in rest_across(False) + rest_beside(False) + rest_facing(False):
+            copy.wait_send()
 
 
 def layer(sp_count, tp_count, cap, operands):
@@ -787,8 +828,8 @@
         (4, sp_count),
         (2,),
         (sp_count // 2,),
-        (3, 2),
-        (3, 2),
+        (9,),
+        (9,),
         (4,),
         (2, sp_count),
         (1,),

time: 91.6 us -> 89.8 us (0.980)
  Pallas kernels: 90.5 us -> 89 us
    pallas_call x1, Pallas kernels: 87.6 us -> 86.2 us  [layer(): pl.pallas_call(grouped, out_shape=[pltpu.VMEM(shape, exact) for shape in...]
where the time goes in v2:
time: 89.8 us; the launch traced here: 89.7 us
  Pallas kernels  89 us (99%)
    pallas_call x1, Pallas kernels, layer(): pl.pallas_call(grouped, out_shape=[pltpu.VMEM(shape, exact) for shape in...  86.2 us
    pallas_call x1, Pallas kernels, store(): pl.pallas_call(store_kernel, out_shape=[jax.ShapeDtypeStruct(value.shape,...  2.88 us

profile of v2, /device:TPU:0, one launch (start us, length us, event | category | flops | bytes accessed | tf_op | source)
XLA Modules:
  0.0 89.7 jit_solution(5055061716712502046)
XLA Ops:
  0.6 86.2 %shard_map.190 = (f32[2048,256]{1,0:T(8,128)S(1)}, f32[2048,256]{1,0:T(8,128)S(1)}, f32[256,2048]{1,0:T(8,128)S(1)}, f32[256,256]{1,0:T(8,128)S(1)}, f32[192,256]{1,0:T(8,128)S(1)}, /*index=5*/f32[192,256]{1,0:T(8,128)S(1)}) custom-call(bf16[192,2048]{1,0:T(8,128)(2,1)} %refs_0_.1, bf16[192,2048]{1,0:T(8,128)(2,1)} %refs_1_.1, f32[1,2048]{1,0:T(1,128)} %bitcast.13, ...), custom_call_target="tpu_custom_call" | custom-call | bytes 40000000 | tf_op jit(solution)/shard_map/pallas_call | solution.py:841
  86.8 2.9 %shard_map.191 = (f32[2048,256]{1,0:T(8,128)}, f32[2048,256]{1,0:T(8,128)}, f32[256,2048]{1,0:T(8,128)}, f32[256,256]{1,0:T(8,128)}, f32[192,256]{1,0:T(8,128)}, /*index=5*/f32[192,256]{1,0:T(8,128)}) custom-call(f32[2048,256]{1,0:T(8,128)S(1)} %get-tuple-element.18.refs_0_, f32[2048,256]{1,0:T(8,128)S(1)} %get-tuple-element.19.refs_1_, ...), custom_call_target="tpu_custom_call" | custom-call | tf_op jit(solution)/shard_map/pallas_call | solution.py:877

commit v3 on v2

--- a/solution.py
+++ b/solution.py
@@ -441,7 +441,6 @@
 
         @pl.when(i == sp_count)
         def _():
-            crossing(2).start()
             crossing(3).start()
 
         @pl.when(i >= near + 3)
@@ -453,10 +452,10 @@
         def _():
             leave(0)
             leave(1)
+            leave(2)
 
         @pl.when(i == sp_count + 1)
         def _():
-            leave(2)
             leave(3)
 
         @pl.when((i >= 1) & (i < sp_count))
@@ -481,6 +480,7 @@
         def _():
             crossing(0).start()
             crossing(1).start()
+            crossing(2).start()
 
         @pl.when((i >= 1) & (i < sp_count + 1))
         def _():

time: 89.8 us -> 91.9 us (1.023)
  Pallas kernels: 89 us -> 91.1 us
    pallas_call x1, Pallas kernels: 86.2 us -> 88.3 us  [layer(): pl.pallas_call(grouped, out_shape=[pltpu.VMEM(shape, exact) for shape in...]
where the time goes in v3:
time: 91.9 us; the launch traced here: 91.8 us
  Pallas kernels  91.1 us (99%)
    pallas_call x1, Pallas kernels, layer(): pl.pallas_call(grouped, out_shape=[pltpu.VMEM(shape, exact) for shape in...  88.3 us
    pallas_call x1, Pallas kernels, store(): pl.pallas_call(store_kernel, out_shape=[jax.ShapeDtypeStruct(value.shape,...  2.88 us

profile of v3, /device:TPU:0, one launch (start us, length us, event | category | flops | bytes accessed | tf_op | source)
XLA Modules:
  0.0 91.8 jit_solution(3565898007198171929)
XLA Ops:
  0.6 88.3 %shard_map.190 = (f32[2048,256]{1,0:T(8,128)S(1)}, f32[2048,256]{1,0:T(8,128)S(1)}, f32[256,2048]{1,0:T(8,128)S(1)}, f32[256,256]{1,0:T(8,128)S(1)}, f32[192,256]{1,0:T(8,128)S(1)}, /*index=5*/f32[192,256]{1,0:T(8,128)S(1)}) custom-call(bf16[192,2048]{1,0:T(8,128)(2,1)} %refs_0_.1, bf16[192,2048]{1,0:T(8,128)(2,1)} %refs_1_.1, f32[1,2048]{1,0:T(1,128)} %bitcast.13, ...), custom_call_target="tpu_custom_call" | custom-call | bytes 40000000 | tf_op jit(solution)/shard_map/pallas_call | solution.py:841
  88.9 2.9 %shard_map.191 = (f32[2048,256]{1,0:T(8,128)}, f32[2048,256]{1,0:T(8,128)}, f32[256,2048]{1,0:T(8,128)}, f32[256,256]{1,0:T(8,128)}, f32[192,256]{1,0:T(8,128)}, /*index=5*/f32[192,256]{1,0:T(8,128)}) custom-call(f32[2048,256]{1,0:T(8,128)S(1)} %get-tuple-element.18.refs_0_, f32[2048,256]{1,0:T(8,128)S(1)} %get-tuple-element.19.refs_1_, ...), custom_call_target="tpu_custom_call" | custom-call | tf_op jit(solution)/shard_map/pallas_call | solution.py:877
